TPU v7x, 32 devices: a whole 2x2x4 slice. The times are simulated.
32 devices in a mesh: rep: 2 (over x), fs: 4 (over z), tp: 4 (over y, core).
Axes of the slice: x: 2, y: 2, z: 4, core: 2. Of those that a mesh axis runs over, the one named last changes fastest.
Arguments:
- tokens: bfloat16 [8192, 1024], P(('rep', 'fs', 'tp')), may hold values from -6 to 6
- norm_gain: float32 [1024], replicated, may hold values from 0.5 to 1.5
- gate_weight: bfloat16 [1024, 3072], P(('rep', 'fs'), 'tp'), may hold values from -0.1875 to 0.1875
- up_weight: bfloat16 [1024, 3072], P(('rep', 'fs'), 'tp'), may hold values from -0.1875 to 0.1875
- down_weight: bfloat16 [3072, 1024], P('tp', ('rep', 'fs')), may hold values from -0.109375 to 0.109375
Outputs:
- block_out: bfloat16 [8192, 1024], P(('rep', 'fs', 'tp'))
All inputs are finite; a program needn't handle non-finite values.
Results may differ from a plain program's by a relative error of at most 0.001.
Values may be sent and summed in bfloat16 or wider, within the bound.
A program may use at most 64 MiB of HBM per device.

v0:
```python
import jax
import jax.numpy as jnp
from jax import lax
from jax.sharding import PartitionSpec as P

epsilon = 1e-06


def over_all(shard, axis, dim, absorb, carry):
    whole = jax.tree.map(lambda part: lax.all_gather(part, axis, axis=dim, tiled=True), shard)
    return absorb(carry, whole, jnp.int32(0))


def summed_rows(portion, width, axis):
    count = width * lax.axis_size(axis)
    return lax.psum_scatter(portion(jnp.int32(0), count), axis, scatter_dimension=0, tiled=True)


def on_device(tokens, norm_gain, gate_weight, up_weight, down_weight):
    values = tokens.astype(jnp.float32)
    inverse_rms = lax.rsqrt(jnp.mean(values * values, axis=-1, keepdims=True) + epsilon)
    normed = (values * inverse_rms * norm_gain.astype(jnp.float32)).astype(jnp.bfloat16)
    gathered = lax.all_gather(normed, "tp", axis=0, tiled=True)
    zero_sums = jnp.zeros((gathered.shape[0], gate_weight.shape[1]), jnp.float32)

    def add_block(running, row_block, first_row):
        columns = lax.dynamic_slice_in_dim(gathered, first_row, row_block.shape[0], 1)
        return running + jnp.dot(columns, row_block, preferred_element_type=jnp.float32)

    gate_value = over_all(gate_weight, ("rep", "fs"), 0, add_block, zero_sums)
    up_value = over_all(up_weight, ("rep", "fs"), 0, add_block, zero_sums)
    hidden = (jax.nn.silu(gate_value) * up_value).astype(jnp.bfloat16)
    own_half = lax.all_gather(down_weight, "fs", axis=1, tiled=True)
    down_whole = lax.all_gather(own_half, "rep", axis=1, tiled=True)
    own_rows = tokens.shape[0]

    def row_terms(first_row, row_count):
        token_block = lax.dynamic_slice_in_dim(hidden, first_row, row_count, 0)
        return jnp.dot(token_block, down_whole, preferred_element_type=jnp.float32)

    mixed_out = summed_rows(row_terms, own_rows, "tp")
    return mixed_out.astype(jnp.bfloat16)


def solution(mesh):
    return jax.shard_map(
        on_device,
        mesh=mesh,
        in_specs=(
            P(("rep", "fs", "tp"), None),
            P(),
            P(("rep", "fs"), "tp"),
            P(("rep", "fs"), "tp"),
            P("tp", ("rep", "fs")),
        ),
        out_specs=P(("rep", "fs", "tp"), None),
        check_vma=False,
    )
```

profile of v0, /device:TPU:0, one launch (start us, length us, event | category | flops | bytes accessed | tf_op | source)
XLA Modules:
  0.0 218.2 jit_solution(9125715528160293608)
XLA Ops:
  6.5 0.0 copy-start
  6.5 0.0 all-gather.7.cloned.1.call-start
  6.5 0.7 all-gather.7.cloned.1.call-update
  7.3 0.0 all-gather.5.cloned.1.call-start
  7.3 1.2 fusion.1
  8.5 2.0 fusion.3
  10.6 0.0 all-gather.5.cloned.1.call-update
  10.6 0.0 all-gather.11.cloned.1.call-start
  10.6 0.0 copy-done
  10.7 26.2 %all_gather.18 = bf16[768,512]{1,0:T(8,128)(2,1)} all-gather(bf16[768,128]{1,0:T(8,128)(2,1)S(1)} %copy-done), channel_id=1, replica_groups=mesh['rep'=2,'fs'=4,'tp'=4] {'fs'}, dimensions={1}, use_global_device_ids=true | all-gather | bytes 983040 | tf_op jit(solution)/shard_map/all_gather | solution.py:33
  36.8 0.0 all-gather.11.cloned.1.call-update
  36.9 0.0 all-gather.9.cloned.1.call-start
  36.9 0.5 all-gather.9.cloned.1.call-update
  37.5 0.0 reduce-scatter.2.cloned.1.call-start
  37.5 22.4 %all-gather.7.cloned.1.call-done = bf16[1024,768]{1,0:T(8,128)(2,1)} async-done(((bf16[128,768]{1,0:T(8,128)(2,1)}), bf16[1024,768]{1,0:T(8,128)(2,1)}) %all-gather.7.cloned.1.call-update) | async-done | bytes 1572880 | tf_op jit(solution)/shard_map/all_gather | solution.py:10
  59.9 22.5 %all-gather.5.cloned.1.call-done = bf16[1024,1024]{1,0:T(8,128)(2,1)} async-done(((bf16[256,1024]{1,0:T(8,128)(2,1)}), bf16[1024,1024]{1,0:T(8,128)(2,1)}) %all-gather.5.cloned.1.call-update) | async-done | bytes 2097168 | tf_op jit(solution)/shard_map/all_gather | solution.py:23
  82.4 0.0 copy-start.1
  82.4 5.6 %fusion.5 = f32[1024,768]{1,0:T(8,128)} fusion(bf16[1024,1024]{1,0:T(8,128)(2,1)} %all-gather.5.cloned.1.call-done, bf16[1024,768]{1,0:T(8,128)(2,1)} %all-gather.7.cloned.1.call-done), kind=kOutput, calls=%fused_computation.9 | convolution fusion | flops 1610612736 | bytes 6815744 | tf_op jit(solution)/shard_map/dot_general | solution.py:28
  88.0 23.1 %all-gather.11.cloned.1.call-done = bf16[768,1024]{1,0:T(8,128)(2,1)} async-done(((bf16[768,512]{1,0:T(8,128)(2,1)}), bf16[768,1024]{1,0:T(8,128)(2,1)}) %all-gather.11.cloned.1.call-update) | async-done | bytes 1572880 | tf_op jit(solution)/shard_map/all_gather | solution.py:34
  111.2 46.2 %all-gather.9.cloned.1.call-done = bf16[1024,768]{1,0:T(8,128)(2,1)} async-done(((bf16[128,768]{1,0:T(8,128)(2,1)}), bf16[1024,768]{1,0:T(8,128)(2,1)}) %all-gather.9.cloned.1.call-update) | async-done | bytes 1572880 | tf_op jit(solution)/shard_map/all_gather | solution.py:10
  157.3 0.0 copy-done.1
  157.3 9.1 %fusion = f32[1024,1024]{1,0:T(8,128)} fusion(bf16[768,1024]{1,0:T(8,128)(2,1)} %all-gather.11.cloned.1.call-done, f32[1024,768]{1,0:T(8,128)} %fusion.5, bf16[1024,1024]{1,0:T(8,128)(2,1)S(1)} %copy-done.1, bf16[1024,768]{1,0:T(8,128)(2,1)} %all-gather.9.cloned.1.call-done), kind=kOutput, calls=%fused_computation.1 | convolution fusion | flops 3225944064 | bytes 12582912 | tf_op jit(solution)/shard_map/dot_general | solution.py:39
  166.5 0.0 reduce-scatter.2.cloned.1.call-update
  166.5 43.1 %reduce-scatter.2.cloned.1.call-done = f32[256,1024]{1,0:T(8,128)} async-done(((f32[1024,1024]{1,0:T(8,128)}), f32[256,1024]{1,0:T(8,128)}) %reduce-scatter.2.cloned.1.call-update) | async-done | bytes 1048592 | tf_op jit(solution)/shard_map/reduce_scatter | solution.py:16
  209.6 2.1 convert_element_type.15
  (1 shorter events, 0.0 us)
Async XLA Ops:
  6.5 4.1 %copy-start = (bf16[768,128]{1,0:T(8,128)(2,1)S(1)}, bf16[768,128]{1,0:T(8,128)(2,1)}, u32[]{:S(2)}) copy-start(bf16[768,128]{1,0:T(8,128)(2,1)} %param.9) | copy-start | bytes 589828
  6.5 53.3 %all-gather.7.cloned.1.call-start = ((), (), s32[]{:S(2)}) async-start(), calls=%async_computation.2 | async-start | bytes 1769472 | tf_op jit(solution)/shard_map/all_gather | solution.py:10
  7.3 75.1 %all-gather.5.cloned.1.call-start = ((), (), s32[]{:S(2)}) async-start(), calls=%async_computation.1 | async-start | bytes 2621440 | tf_op jit(solution)/shard_map/all_gather | solution.py:23
  10.6 100.6 %all-gather.11.cloned.1.call-start = ((), (), s32[]{:S(2)}) async-start(), calls=%async_computation.4 | async-start | bytes 2359296 | tf_op jit(solution)/shard_map/all_gather | solution.py:34
  36.9 120.5 %all-gather.9.cloned.1.call-start = ((), (), s32[]{:S(2)}) async-start(), calls=%async_computation.3 | async-start | bytes 1769472 | tf_op jit(solution)/shard_map/all_gather | solution.py:10
  37.5 172.1 %reduce-scatter.2.cloned.1.call-start = ((), (), s32[]{:S(2)}) async-start(), calls=%async_computation.5 | async-start | bytes 5242880 | tf_op jit(solution)/shard_map/reduce_scatter | solution.py:16
  82.4 74.9 %copy-start.1 = (bf16[1024,1024]{1,0:T(8,128)(2,1)S(1)}, bf16[1024,1024]{1,0:T(8,128)(2,1)}, u32[]{:S(2)}) copy-start(bf16[1024,1024]{1,0:T(8,128)(2,1)} %all-gather.5.cloned.1.call-done) | copy-start | bytes 6291460
Sparse Core Ops, SparseCore 0:
  9.4 50.3 all-gather.6
  61.4 20.9 all-gather.4
  83.9 27.1 all-gather.10
  113.1 44.1 all-gather.8
  166.6 42.9 reduce-scatter.1
where the time goes:
time: 218 us
  waiting for transfers between devices  159 us (73%)
  blocking collectives  26.2 us (12%)
  matrix products  14.8 us (7%)
  between operations  13.2 us (6%)
  other arithmetic  5.36 us (2%)
    all_gather x2, waiting for transfers between devices, over_all(): lax.all_gather(part, axis, axis=dim, tiled=True)  68.5 us
    reduce_scatter x1, waiting for transfers between devices, summed_rows(): lax.psum_scatter(portion(jnp.int32(0), count), axis, scatter_dimension=0,...  43.1 us
    all_gather x1, blocking collectives, on_device(): own_half = lax.all_gather(down_weight, 'fs', axis=1, tiled=True)  26.2 us
    all_gather x1, waiting for transfers between devices, on_device(): down_whole = lax.all_gather(own_half, 'rep', axis=1, tiled=True)  23.1 us
    all_gather x1, waiting for transfers between devices, on_device(): gathered = lax.all_gather(normed, 'tp', axis=0, tiled=True)  22.5 us
    dot_general x1, matrix products, row_terms(): return jnp.dot(token_block, down_whole, preferred_element_type=jnp.float32)  9.14 us
    dot_general x1, matrix products, add_block(): jnp.dot(columns, row_block, preferred_element_type=jnp.float32)  5.65 us
  transfers between devices with their start and end apart: 5, of which 5 were waited for; matrix products, arithmetic and copies ran while one was open for 4% of the time, Pallas kernels for 0%

commit v1 on v0

--- a/solution.py
+++ b/solution.py
@@ -20,7 +20,12 @@
     values = tokens.astype(jnp.float32)
     inverse_rms = lax.rsqrt(jnp.mean(values * values, axis=-1, keepdims=True) + epsilon)
     normed = (values * inverse_rms * norm_gain.astype(jnp.float32)).astype(jnp.bfloat16)
-    gathered = lax.all_gather(normed, "tp", axis=0, tiled=True)
+    ring = [normed]
+    for hop in range(3):
+        ring.append(lax.ppermute(ring[-1], "tp", [(dev, (dev + 1) % 4) for dev in range(4)]))
+    gathered = jnp.roll(
+        jnp.concatenate(ring[::-1], axis=0), (lax.axis_index("tp") + 1) * ring[0].shape[0], axis=0
+    )
     zero_sums = jnp.zeros((gathered.shape[0], gate_weight.shape[1]), jnp.float32)
 
     def add_block(running, row_block, first_row):

time: 218 us -> 195 us (0.89)
  waiting for transfers between devices: 159 us -> 129 us
  local copies, waits for them, and re-layouts: 0.01 us -> 5.04 us
    ppermute x0 -> x3, waiting for transfers between devices: none -> 25.7 us  [on_device(): lax.ppermute(ring[-1], 'tp', [(dev, (dev + 1) % 4) for dev in range(4)])]
    all_gather x1 -> x0, waiting for transfers between devices: 22.5 us -> none  [on_device(): gathered = lax.all_gather(normed, 'tp', axis=0, tiled=True)]
    all_gather x2, waiting for transfers between devices: 68.5 us -> 46.3 us  [over_all(): lax.all_gather(part, axis, axis=dim, tiled=True)]
    all_gather x1, waiting for transfers between devices: 23.1 us -> 12.9 us  [on_device(): down_whole = lax.all_gather(own_half, 'rep', axis=1, tiled=True)]
    unnamed x4 -> x10, local copies, waits for them, and re-layouts: 0.01 us -> 5.04 us
  transfers between devices with their start and end apart: 5 -> 7, of which waited for: 5 -> 6; matrix products, arithmetic and copies ran while one was open for 4% -> 8% of each run, Pallas kernels for 0% -> 0%
where the time goes in v1:
time: 195 us; the launch traced here: 194 us
  waiting for transfers between devices  129 us (66%)
  blocking collectives  25.3 us (13%)
  matrix products  15.3 us (8%)
  between operations  13.2 us (7%)
  other arithmetic  6.57 us (3%)
  local copies, waits for them, and re-layouts  5.04 us (3%)
    all_gather x2, waiting for transfers between devices, over_all(): lax.all_gather(part, axis, axis=dim, tiled=True)  46.3 us
    reduce_scatter x1, waiting for transfers between devices, summed_rows(): lax.psum_scatter(portion(jnp.int32(0), count), axis, scatter_dimension=0,...  43.1 us
    ppermute x3, waiting for transfers between devices, on_device(): lax.ppermute(ring[-1], 'tp', [(dev, (dev + 1) % 4) for dev in range(4)])  25.7 us
    all_gather x1, blocking collectives, on_device(): own_half = lax.all_gather(down_weight, 'fs', axis=1, tiled=True)  25.3 us
    all_gather x1, waiting for transfers between devices, on_device(): down_whole = lax.all_gather(own_half, 'rep', axis=1, tiled=True)  12.9 us
    dot_general x1, matrix products, row_terms(): return jnp.dot(token_block, down_whole, preferred_element_type=jnp.float32)  9.74 us
    dot_general x1, matrix products, add_block(): jnp.dot(columns, row_block, preferred_element_type=jnp.float32)  5.56 us
    unnamed x10, local copies, waits for them, and re-layouts  5.04 us
  transfers between devices with their start and end apart: 7, of which 6 were waited for; matrix products, arithmetic and copies ran while one was open for 8% of the time, Pallas kernels for 0%

profile of v1, /device:TPU:0, one launch (start us, length us, event | category | flops | bytes accessed | tf_op | source)
XLA Modules:
  0.0 194.4 jit_solution(4105377079536200949)
XLA Ops:
  6.5 0.0 copy-start
  6.5 0.0 copy-start.1
  6.5 0.0 all-gather.6.cloned.1.call-start
  6.5 0.7 all-gather.6.cloned.1.call-update
  7.3 0.0 all-gather.8.cloned.1.call-start
  7.3 25.3 %all_gather.14 = bf16[768,512]{1,0:T(8,128)(2,1)} all-gather(bf16[768,128]{1,0:T(8,128)(2,1)} %param.9), channel_id=1, replica_groups=mesh['rep'=2,'fs'=4,'tp'=4] {'fs'}, dimensions={1}, use_global_device_ids=true | all-gather | bytes 983040 | tf_op jit(solution)/shard_map/all_gather | solution.py:38
  32.6 0.0 all-gather.8.cloned.1.call-update
  32.6 0.0 all-gather.4.cloned.1.call-start
  32.7 1.2 fusion.9
  33.9 1.2 fusion.11
  35.2 0.1 collective-permute-start
  35.2 0.0 all-gather.4.cloned.1.call-update
  35.3 0.0 reduce-scatter.2.cloned.1.call-start
  35.3 8.5 %collective-permute-done = bf16[256,1024]{1,0:T(8,128)(2,1)S(1)} collective-permute-done((bf16[256,1024]{1,0:T(8,128)(2,1)S(1)}, bf16[256,1024]{1,0:T(8,128)(2,1)S(1)}, u32[]{:S(2)}, u32[]{:S(2)}) %collective-permute-start) | collective-permute-done | bytes 524320 | tf_op jit(solution)/shard_map/ppermute | solution.py:25
  43.8 0.0 collective-permute-start.1
  43.8 8.6 %collective-permute-done.1 = bf16[256,1024]{1,0:T(8,128)(2,1)S(1)} collective-permute-done((bf16[256,1024]{1,0:T(8,128)(2,1)S(1)}, bf16[256,1024]{1,0:T(8,128)(2,1)S(1)}, u32[]{:S(2)}, u32[]{:S(2)}) %collective-permute-start.1) | collective-permute-done | bytes 524320 | tf_op jit(solution)/shard_map/ppermute | solution.py:25
  52.4 0.0 collective-permute-start.2
  52.4 8.6 %collective-permute-done.2 = bf16[256,1024]{1,0:T(8,128)(2,1)S(1)} collective-permute-done((bf16[256,1024]{1,0:T(8,128)(2,1)S(1)}, bf16[256,1024]{1,0:T(8,128)(2,1)S(1)}, u32[]{:S(2)}, u32[]{:S(2)}) %collective-permute-start.2) | collective-permute-done | bytes 524320 | tf_op jit(solution)/shard_map/ppermute | solution.py:25
  61.0 0.8 constant_dynamic-update-slice_fusion.7
  61.9 0.8 constant_dynamic-update-slice_fusion.6
  62.7 0.9 constant_dynamic-update-slice_fusion.5
  63.6 0.0 copy-done
  63.6 0.0 copy-done.1
  63.6 1.0 constant_dynamic-update-slice_fusion.4
  64.6 0.8 constant_dynamic-update-slice_fusion.3
  65.4 0.8 constant_dynamic-update-slice_fusion.2
  66.2 0.8 constant_dynamic-update-slice_fusion.1
  67.1 1.0 constant_dynamic-update-slice_fusion
  68.1 0.0 all-gather.6.cloned.1.call-done
  68.1 5.6 %fusion = f32[1024,768]{1,0:T(8,128)} fusion(bf16[1024,768]{1,0:T(8,128)(2,1)} %all-gather.6.cloned.1.call-done, bf16[2048,1024]{1,0:T(8,128)(2,1)} %constant_dynamic-update-slice_fusion, s32[]{:T(128)S(6)} %select_n.14), kind=kOutput, calls=%fused_computation.1 | convolution fusion | flops 1610612736 | bytes 6815748 | tf_op jit(solution)/shard_map/dot_general | solution.py:33
  73.7 12.9 %all-gather.8.cloned.1.call-done = bf16[768,1024]{1,0:T(8,128)(2,1)} async-done(((bf16[768,512]{1,0:T(8,128)(2,1)}), bf16[768,1024]{1,0:T(8,128)(2,1)}) %all-gather.8.cloned.1.call-update) | async-done | bytes 1572880 | tf_op jit(solution)/shard_map/all_gather | solution.py:39
  86.6 46.3 %all-gather.4.cloned.1.call-done = bf16[1024,768]{1,0:T(8,128)(2,1)} async-done(((bf16[128,768]{1,0:T(8,128)(2,1)}), bf16[1024,768]{1,0:T(8,128)(2,1)}) %all-gather.4.cloned.1.call-update) | async-done | bytes 1572880 | tf_op jit(solution)/shard_map/all_gather | solution.py:10
  132.9 9.7 %fusion.4 = f32[1024,1024]{1,0:T(8,128)} fusion(bf16[768,1024]{1,0:T(8,128)(2,1)} %all-gather.8.cloned.1.call-done, f32[1024,768]{1,0:T(8,128)} %fusion, bf16[1024,768]{1,0:T(8,128)(2,1)} %all-gather.4.cloned.1.call-done, bf16[2048,1024]{1,0:T(8,128)(2,1)} %constant_dynamic-update-slice_fusion, s32[]{:T(128)S(6)} %select_n.14), kind=kOutput, calls=%fused_computation.5 | convolution fusion | flops 3225944064 | bytes 12582916 | tf_op jit(solution)/shard_map/dot_general | solution.py:44
  142.6 0.0 reduce-scatter.2.cloned.1.call-update
  142.7 43.1 %reduce-scatter.2.cloned.1.call-done = f32[256,1024]{1,0:T(8,128)} async-done(((f32[1024,1024]{1,0:T(8,128)}), f32[256,1024]{1,0:T(8,128)}) %reduce-scatter.2.cloned.1.call-update) | async-done | bytes 1048592 | tf_op jit(solution)/shard_map/reduce_scatter | solution.py:16
  185.8 2.1 %convert_element_type.15 = bf16[256,1024]{1,0:T(8,128)(2,1)} convert(f32[256,1024]{1,0:T(8,128)} %reduce-scatter.2.cloned.1.call-done) | non-fusion elementwise | flops 262144 | bytes 1572864 | tf_op jit(solution)/shard_map/convert_element_type | solution.py:47
  (1 shorter events, 0.0 us)
Async XLA Ops:
  6.5 57.0 %copy-start = (bf16[256,1024]{1,0:T(8,128)(2,1)S(1)}, bf16[256,1024]{1,0:T(8,128)(2,1)}, u32[]{:S(2)}) copy-start(bf16[256,1024]{1,0:T(8,128)(2,1)} %param.5) | copy-start | bytes 1572868
  6.5 57.0 %copy-start.1 = (f32[1024]{0:T(1024)S(1)}, f32[1024]{0:T(1024)}, u32[]{:S(2)}) copy-start(f32[1024]{0:T(1024)} %param.6) | copy-start | bytes 12292
  6.5 61.6 %all-gather.6.cloned.1.call-start = ((), (), s32[]{:S(2)}) async-start(), calls=%async_computation.2 | async-start | bytes 1769472 | tf_op jit(solution)/shard_map/all_gather | solution.py:10
  7.3 79.3 %all-gather.8.cloned.1.call-start = ((), (), s32[]{:S(2)}) async-start(), calls=%async_computation.3 | async-start | bytes 2359296 | tf_op jit(solution)/shard_map/all_gather | solution.py:39
  32.6 100.2 %all-gather.4.cloned.1.call-start = ((), (), s32[]{:S(2)}) async-start(), calls=%async_computation.1 | async-start | bytes 1769472 | tf_op jit(solution)/shard_map/all_gather | solution.py:10
  35.2 8.7 %collective-permute-start = (bf16[256,1024]{1,0:T(8,128)(2,1)S(1)}, bf16[256,1024]{1,0:T(8,128)(2,1)S(1)}, u32[]{:S(2)}, u32[]{:S(2)}) collective-permute-start(bf16[256,1024]{1,0:T(8,128)(2,1)S(1)} %fusion.11), channel_id=1, source_target_pairs={{0,1},{1,2},{2,3},{3,0},{4,5},{5,6},{6,7},{7,4},{8,9},{9,10},{10,1... | collective-permute-start | bytes 1572872 | tf_op jit(solution)/shard_map/ppermute | solution.py:25
  35.3 150.5 %reduce-scatter.2.cloned.1.call-start = ((), (), s32[]{:S(2)}) async-start(), calls=%async_computation.4 | async-start | bytes 5242880 | tf_op jit(solution)/shard_map/reduce_scatter | solution.py:16
  43.8 8.6 %collective-permute-start.1 = (bf16[256,1024]{1,0:T(8,128)(2,1)S(1)}, bf16[256,1024]{1,0:T(8,128)(2,1)S(1)}, u32[]{:S(2)}, u32[]{:S(2)}) collective-permute-start(bf16[256,1024]{1,0:T(8,128)(2,1)S(1)} %collective-permute-done), channel_id=1, source_target_pairs={{0,1},{1,2},{2,3},{3,0},{4,5},{5,6},{6,7},{7,4},{8,9},{9,10},{10,1... | collective-permute-start | bytes 1572872 | tf_op jit(solution)/shard_map/ppermute | solution.py:25
  52.4 8.6 %collective-permute-start.2 = (bf16[256,1024]{1,0:T(8,128)(2,1)S(1)}, bf16[256,1024]{1,0:T(8,128)(2,1)S(1)}, u32[]{:S(2)}, u32[]{:S(2)}) collective-permute-start(bf16[256,1024]{1,0:T(8,128)(2,1)S(1)} %collective-permute-done.1), channel_id=1, source_target_pairs={{0,1},{1,2},{2,3},{3,0},{4,5},{5,6},{6,7},{7,4},{8,9},{9,10},{10,1... | collective-permute-start | bytes 1572872 | tf_op jit(solution)/shard_map/ppermute | solution.py:25
Sparse Core Ops, SparseCore 0:
  9.4 49.9 all-gather.5
  61.0 25.5 all-gather.7
  88.7 44.1 all-gather.3
  142.8 42.9 reduce-scatter.1
